TPU v7x, 32 devices: a whole 2x2x4 slice. The times are simulated.
32 devices in a mesh: sp: 8 (over z, y), tp: 4 (over x, core).
Axes of the slice: x: 2, y: 2, z: 4, core: 2. Of those that a mesh axis runs over, the one named last changes fastest.
Arguments:
- tokens: bfloat16 [4096, 2048], P('sp', 'tp'), may hold values from -6 to 6
- in_gain: float32 [2048], replicated, may hold values from 0.1 to 1.9
- conv_value_w: bfloat16 [2048, 1024], P(None, 'tp'), may hold values from -0.125 to 0.125
- conv_gate_w: bfloat16 [2048, 1024], P(None, 'tp'), may hold values from -0.125 to 0.125
- conv_taps: float32 [31, 1024], P(None, 'tp'), may hold values from -8 to 8
- conv_gain: float32 [1024], P('tp'), may hold values from 0.1 to 1.9
- query_latent_weight: bfloat16 [2048, 512], replicated, may hold values from -0.125 to 0.125
- latent_weight: bfloat16 [2048, 512], replicated, may hold values from -0.125 to 0.125
- rope_key_w: bfloat16 [2048, 64], replicated, may hold values from -0.125 to 0.125
- query_gain: float32 [512], replicated, may hold values from 1.5 to 8, as said below
- latent_gain: float32 [512], replicated, may hold values from 1.5 to 8, as said below
- query_weight: bfloat16 [512, 1024], P(None, 'tp'), may hold values from -0.25 to 0.25
- query_rotary_weight: bfloat16 [512, 512], P(None, 'tp'), may hold values from -0.25 to 0.25
- key_weight: bfloat16 [512, 1024], P(None, 'tp'), may hold values from -0.25 to 0.25
- value_weight: bfloat16 [512, 1024], P(None, 'tp'), may hold values from -0.25 to 0.25
- conv_out_w: bfloat16 [1024, 2048], P('tp'), may hold values from -0.125 to 0.125
- attn_out_w: bfloat16 [1024, 2048], P('tp'), may hold values from -0.125 to 0.125
- out_gain: float32 [2048], replicated, may hold values from 0.1 to 1.9
Outputs:
- mixed: bfloat16 [4096, 2048], P(('sp', 'tp'))
Inputs may be any that keep to these rules, and one draw needn't show every extreme that they name: `query_gain`: positive gains. `latent_gain`: positive gains.
All inputs are finite; a program needn't handle non-finite values.
Results may differ from a plain program's by a relative error of at most 0.018.
The roundings to bfloat16 on the way count: a program that leaves them out, or rounds other values in their place, can miss the bound.
Values may be sent and summed in bfloat16 or wider, within the bound.
A program may use at most 128 MiB of HBM per device.

v0:
```python
import math

import jax
import jax.numpy as jnp
from jax import lax
from jax.sharding import PartitionSpec as P

CONV_CH = 1024
HEAD_WIDTH = 128


norm_eps = 1e-06
layer_eps = 1e-05
rope_base = 10000.0
block_limit = 512


def extended(value, sides, width):
    for axis, dim in sides:
        size, length = (lax.axis_size(axis), value.shape[dim])
        up = [(i, (i + 1) % size) for i in range(size - 1)]
        down = [(j, i) for i, j in up]
        last = lax.slice_in_dim(value, length - width, length, axis=dim)
        leading = lax.slice_in_dim(value, 0, width, axis=dim)
        before = lax.ppermute(last, axis, up)
        after = lax.ppermute(leading, axis, down)
        value = jnp.concatenate([before, value, after], axis=dim)
    return value


def rms_scaled(values, gain):
    return values * lax.rsqrt(jnp.mean(values * values, axis=-1, keepdims=True) + norm_eps) * gain


def rotate(values, cosine_table, sine_table):
    halfway = values.shape[-1] // 2
    first = values[..., :halfway]
    second = values[..., halfway:]
    return jnp.concatenate(
        [first * cosine_table - second * sine_table, second * cosine_table + first * sine_table],
        axis=-1,
    )


def tables(positions, width):
    halfway = width // 2
    inverse = rope_base ** (-jnp.arange(halfway, dtype=jnp.float32) / halfway)
    angles = positions[:, None] * inverse[None, :]
    return (jnp.cos(angles), jnp.sin(angles))


def local(
    tokens,
    in_gain,
    conv_value_w,
    conv_gate_w,
    conv_taps,
    conv_gain,
    query_latent_weight,
    latent_weight,
    rope_key_w,
    query_gain,
    latent_gain,
    query_weight,
    query_rotary_weight,
    key_weight,
    value_weight,
    conv_out_w,
    attn_out_w,
    out_gain,
):
    full_rows = lax.all_gather(tokens, "tp", axis=1, tiled=True)
    tok_here = full_rows.shape[0]
    normed = rms_scaled(full_rows.astype(jnp.float32), in_gain).astype(jnp.bfloat16)
    conv_value = jnp.dot(normed, conv_value_w, preferred_element_type=jnp.float32)
    conv_gate = jnp.dot(normed, conv_gate_w, preferred_element_type=jnp.float32)
    gated = (conv_value * jax.nn.sigmoid(conv_gate)).astype(jnp.bfloat16)
    reach = conv_taps.shape[0] // 2
    padded = extended(gated, (("sp", 0),), reach).astype(jnp.float32)
    convolved = jnp.zeros(gated.shape, jnp.float32)
    for offset_tap in range(conv_taps.shape[0]):
        convolved = convolved + conv_taps[offset_tap] * padded[offset_tap : offset_tap + tok_here]
    stat_sums = lax.psum((jnp.sum(convolved, axis=1), jnp.sum(convolved * convolved, axis=1)), "tp")
    chan_mean = stat_sums[0] / CONV_CH
    chan_square = stat_sums[1] / CONV_CH
    shaped = (
        (convolved - chan_mean[:, None])
        * lax.rsqrt(chan_square - chan_mean * chan_mean + layer_eps)[:, None]
        * conv_gain
    )
    conv_result = jax.nn.silu(shaped).astype(jnp.bfloat16)
    rope_width = rope_key_w.shape[1]
    heads_here = key_weight.shape[1] // HEAD_WIDTH
    score_scale = (HEAD_WIDTH + rope_width) ** (-0.5)
    positions = (lax.axis_index("sp") * tok_here + jnp.arange(tok_here, dtype=jnp.int32)).astype(
        jnp.float32
    )
    cosine_table, sine_table = tables(positions, rope_width)
    query_lat = rms_scaled(
        jnp.dot(normed, query_latent_weight, preferred_element_type=jnp.float32), query_gain
    ).astype(jnp.bfloat16)
    latent = rms_scaled(
        jnp.dot(normed, latent_weight, preferred_element_type=jnp.float32), latent_gain
    ).astype(jnp.bfloat16)
    rope_keys = rotate(
        jnp.dot(normed, rope_key_w, preferred_element_type=jnp.float32), cosine_table, sine_table
    ).astype(jnp.bfloat16)
    query_main = (
        jnp.dot(query_lat, query_weight, preferred_element_type=jnp.float32)
        .astype(jnp.bfloat16)
        .reshape(tok_here, heads_here, HEAD_WIDTH)
    )
    query_rope = rotate(
        jnp.dot(query_lat, query_rotary_weight, preferred_element_type=jnp.float32).reshape(
            tok_here, heads_here, rope_width
        ),
        cosine_table[:, None, :],
        sine_table[:, None, :],
    ).astype(jnp.bfloat16)

    def attend(state, key_rows, rope_rows, value_rows):
        running_max, running_sum, accum = state
        scores = (
            jnp.einsum("thd,phd->htp", query_main, key_rows, preferred_element_type=jnp.float32)
            + jnp.einsum("thr,pr->htp", query_rope, rope_rows, preferred_element_type=jnp.float32)
        ) * score_scale
        new_max = jnp.maximum(running_max, jnp.max(scores, axis=-1))
        rescale = jnp.exp(running_max - new_max)
        weights = jnp.exp(scores - new_max[:, :, None])
        running_sum = running_sum * rescale + jnp.sum(weights, axis=-1)
        accum = accum * rescale.T[:, :, None] + jnp.einsum(
            "htp,phd->thd",
            weights.astype(jnp.bfloat16),
            value_rows,
            preferred_element_type=jnp.float32,
        )
        return (new_max, running_sum, accum)

    start_state = (
        jnp.full((heads_here, tok_here), -1e30, jnp.float32),
        jnp.zeros((heads_here, tok_here), jnp.float32),
        jnp.zeros((tok_here, heads_here, HEAD_WIDTH), jnp.float32),
    )
    state = start_state
    arrays = (
        lax.all_gather(latent, "sp", axis=0, tiled=True),
        lax.all_gather(rope_keys, "sp", axis=0, tiled=True),
    )
    count = arrays[0].shape[0]
    block_rows = math.gcd(count, block_limit)
    stacked = tuple(
        (member.reshape((count // block_rows, block_rows) + member.shape[1:]) for member in arrays)
    )

    def block_step(inner, pieces):
        latent_rows, rope_rows = pieces
        key_rows = jnp.dot(latent_rows, key_weight, preferred_element_type=jnp.float32).astype(
            jnp.bfloat16
        )
        value_flat = jnp.dot(latent_rows, value_weight, preferred_element_type=jnp.float32).astype(
            jnp.bfloat16
        )
        key_rows = key_rows.reshape(block_rows, heads_here, HEAD_WIDTH)
        value_rows = value_flat.reshape(block_rows, heads_here, HEAD_WIDTH)
        return (attend(inner, key_rows, rope_rows, value_rows), None)

    state, unused = lax.scan(block_step, state, stacked)
    running_max, running_sum, accum = state
    attention_result = (
        (accum / running_sum.T[:, :, None])
        .astype(jnp.bfloat16)
        .reshape(tok_here, heads_here * HEAD_WIDTH)
    )
    summed = jnp.dot(conv_result, conv_out_w, preferred_element_type=jnp.float32) + jnp.dot(
        attention_result, attn_out_w, preferred_element_type=jnp.float32
    )
    merged = lax.psum_scatter(
        lax.optimization_barrier(summed.astype(jnp.bfloat16))
        .astype(jnp.float32)
        .astype(jnp.bfloat16),
        "tp",
        scatter_dimension=0,
        tiled=True,
    ).astype(jnp.float32)
    return rms_scaled(merged, out_gain).astype(jnp.bfloat16)


def solution(mesh):
    return jax.shard_map(
        local,
        mesh=mesh,
        in_specs=(
            P("sp", "tp"),
            P(),
            P(None, "tp"),
            P(None, "tp"),
            P(None, "tp"),
            P("tp"),
            P(),
            P(),
            P(),
            P(),
            P(),
            P(None, "tp"),
            P(None, "tp"),
            P(None, "tp"),
            P(None, "tp"),
            P("tp", None),
            P("tp", None),
            P(),
        ),
        out_specs=P(("sp", "tp"), None),
        check_vma=False,
    )
```

profile of v0, /device:TPU:0, one launch (start us, length us, event | category | flops | bytes accessed | tf_op | source)
XLA Modules:
  0.0 212.8 jit_solution(5674878979856486515)
XLA Ops:
  7.3 26.9 %all-gather.3.cloned.1.call-done = bf16[512,2048]{1,0:T(8,128)(2,1)} async-done(((bf16[512,512]{1,0:T(8,128)(2,1)}), bf16[512,2048]{1,0:T(8,128)(2,1)}) %all-gather.3.cloned.1.call-update) | async-done | bytes 2097168 | tf_op jit(solution)/shard_map/all_gather | solution.py:72
  34.2 2.2 %fusion.18 = f32[512]{0:T(512)S(1)} fusion(bf16[512,2048]{1,0:T(8,128)(2,1)} %all-gather.3.cloned.1.call-done), kind=kLoop, calls=%fused_computation.28 | loop fusion | flops 3145216 | bytes 2099200 | tf_op jit(solution)/shard_map/reduce_sum | solution.py:32
  36.5 1.4 multiply_reduce_fusion.1
  40.4 2.8 %fusion.23 = f32[512,256]{1,0:T(8,128)S(1)} fusion(bf16[2048,256]{1,0:T(8,128)(2,1)} %param.23, bf16[512,2048]{1,0:T(8,128)(2,1)} %all-gather.3.cloned.1.call-done, f32[2048]{0:T(1024)S(1)} %copy-done.14, f32[512]{0:T(512)S(1)} %add_rsqrt_fusion.3), kind=kOutput, calls=%fused_computation.38 | convolution fusion | flops 541458432 | bytes 3680256 | tf_op jit(solution)/shard_map/dot_general | solution.py:76
  44.6 3.4 %collective-permute-start = (bf16[15,256]{1,0:T(8,128)(2,1)}, bf16[15,256]{1,0:T(8,128)(2,1)S(1)}, u32[]{:S(2)}, u32[]{:S(2)}) collective-permute-start(bf16[15,256]{1,0:T(8,128)(2,1)} %get-tuple-element.134), channel_id=1, source_target_pairs={{0,4},{4,8},{8,12},{12,16},{16,20},{20,24},{24,28},{1,5},{5,9},{9,... | collective-permute-start | bytes 23048 | tf_op jit(solution)/shard_map/ppermute | solution.py:25
  48.0 1.4 collective-permute-start.1
  50.7 1.5 multiply_reduce_fusion
  52.2 35.2 %all_gather.11 = bf16[4096,64]{0,1:T(8,128)(2,1)S(1)} all-gather(bf16[512,64]{0,1:T(8,128)(2,1)S(1)} %pad_maximum_fusion.1), channel_id=1, replica_groups=mesh['sp'=8,'tp'=4] {'sp'}, dimensions={0}, use_global_device_ids=true | all-gather | bytes 589824 | tf_op jit(solution)/shard_map/all_gather | solution.py:147
  90.1 3.3 %fusion.73 = (f32[512]{0:T(512)S(1)}, f32[512]{0:T(512)S(1)}, f32[512,256]{1,0:T(8,128)S(1)}) fusion(f32[542,256]{1,0:T(8,128)S(1)} %maximum_convert_fusion, f32[256]{0:T(256)} %bitcast.126, f32[256]{0:T(256)} %bitcast.127, f32[256]{0:T(256)} %bitcast.129, f32[256]{0:T(256)} %bitcast.130, f32[256]{0:T(256)} %bitcast.131, f32[256]{0:T(256)} %bitcast.132, ...), kind=kLoop, calls=%fused_computation.140 | loop fusion | flops 8387584 | bytes 16813056 | tf_op jit(solution)/shard_map/reduce_sum | solution.py:83
  93.5 6.8 %all-reduce = (f32[512]{0:T(512)}, f32[512]{0:T(512)}) all-reduce(f32[512]{0:T(512)S(1)} %get-tuple-element.104, f32[512]{0:T(512)S(1)} %get-tuple-element.103), channel_id=1, replica_groups=mesh['sp'=8,'tp'=4] {'tp'}, use_global_device_ids=true, to_apply=%region_4.0 | all-reduce | flops 1024 | bytes 8192 | tf_op jit(solution)/shard_map/psum | solution.py:83
  101.0 4.0 %fusion.58 = f32[512,2048]{1,0:T(8,128)} fusion(bf16[256,2048]{1,0:T(8,128)(2,1)} %param.35, f32[512,256]{1,0:T(8,128)S(1)} %get-tuple-element.129, f32[256]{0:T(256)} %param.25, f32[512]{0:T(512)S(1)} %get-tuple-element.174, f32[512]{0:T(512)S(1)} %get-tuple-element.173), kind=kOutput, calls=%fused_computation.114 | convolution fusion | flops 537919488 | bytes 5772288 | tf_op jit(solution)/shard_map/dot_general | solution.py:174
  105.0 12.6 %all-gather.5.cloned.1.call-done = bf16[4096,512]{0,1:T(8,128)(2,1)} async-done(((bf16[512,512]{0,1:T(8,128)(2,1)}), bf16[4096,512]{0,1:T(8,128)(2,1)}) %all-gather.5.cloned.1.call-update) | async-done | bytes 4194320 | tf_op jit(solution)/shard_map/all_gather | solution.py:146
  117.6 6.4 %copy.26 = bf16[4096,512]{1,0:T(8,128)(2,1)} copy(bf16[4096,512]{0,1:T(8,128)(2,1)} %all-gather.5.cloned.1.call-done) | data formatting | bytes 8388608
  124.1 44.4 %while.15 = (s32[]{:T(128)}, f32[2,512]{1,0:T(2,128)S(1)}, f32[2,512]{1,0:T(2,128)S(1)}, f32[512,2,128]{0,2,1:T(8,128)S(1)}, bf16[8,512,512]{2,1,0:T(8,128)(2,1)...) while((s32[]{:T(128)}, f32[2,512]{1,0:T(2,128)S(1)}, ...), condition=%wide.region_10.11_spmd.clone, body=%wide.region_7.10_spmd.clone.sunk | while | flops 608311296 | bytes 14680213 | solution.py:167
  124.1 1.4 convolution_convert_fusion.6
  125.5 1.4 convolution_convert_fusion.5
  129.6 1.4 convolution_convert_fusion.6
  131.0 1.4 convolution_convert_fusion.5
  135.2 1.4 convolution_convert_fusion.6
  136.6 1.4 convolution_convert_fusion.5
  140.7 1.4 convolution_convert_fusion.6
  142.1 1.4 convolution_convert_fusion.5
  146.3 1.4 convolution_convert_fusion.6
  147.7 1.4 convolution_convert_fusion.5
  151.8 1.4 convolution_convert_fusion.6
  153.2 1.4 convolution_convert_fusion.5
  157.4 1.4 convolution_convert_fusion.6
  158.8 1.4 convolution_convert_fusion.5
  164.3 1.4 convolution_convert_fusion.5
  168.5 4.6 %add_convert_fusion = bf16[512,2048]{1,0:T(8,128)(2,1)} fusion(f32[512,2048]{1,0:T(8,128)} %fusion.58, bf16[512,256]{0,1:T(8,128)(2,1)S(1)} %bitcast.114, bf16[256,2048]{1,0:T(8,128)(2,1)} %param.36), kind=kOutput, calls=%fused_computation.31 | convolution fusion | flops 538968064 | bytes 7602176 | tf_op jit(solution)/shard_map/dot_general | solution.py:174
  173.1 29.9 %reduce-scatter.2.cloned.1.call-done = bf16[128,2048]{1,0:T(8,128)(2,1)} async-done(((bf16[512,2048]{1,0:T(8,128)(2,1)}), bf16[128,2048]{1,0:T(8,128)(2,1)}) %reduce-scatter.2.cloned.1.call-update) | async-done | bytes 524304 | tf_op jit(solution)/shard_map/reduce_scatter | solution.py:177
  204.3 2.0 fusion.27
  (124 shorter events, 33.4 us)
Async XLA Ops:
  6.5 29.9 %copy-start = (bf16[2048,512]{1,0:T(8,128)(2,1)S(1)}, bf16[2048,512]{1,0:T(8,128)(2,1)}, u32[]{:S(2)}) copy-start(bf16[2048,512]{1,0:T(8,128)(2,1)} %param.27) | copy-start | bytes 6291460
  6.5 29.9 %copy-start.14 = (f32[2048]{0:T(1024)S(1)}, f32[2048]{0:T(1024)}, u32[]{:S(2)}) copy-start(f32[2048]{0:T(1024)} %param.21) | copy-start | bytes 24580
  6.5 27.7 %all-gather.3.cloned.1.call-start = ((), (), s32[]{:S(2)}) async-start(), calls=%async_computation.1 | async-start | bytes 2621440 | tf_op jit(solution)/shard_map/all_gather | solution.py:72
  7.3 110.4 %all-gather.5.cloned.1.call-start = ((), (), s32[]{:S(2)}) async-start(), calls=%async_computation.2 | async-start | bytes 4718592 | tf_op jit(solution)/shard_map/all_gather | solution.py:146
  34.2 2.3 %copy-start.3 = (bf16[512,2048]{1,0:T(8,128)(2,1)S(1)}, bf16[512,2048]{1,0:T(8,128)(2,1)}, u32[]{:S(2)}) copy-start(bf16[512,2048]{1,0:T(8,128)(2,1)} %all-gather.3.cloned.1.call-done) | copy-start | bytes 6291460
  36.5 1.5 copy-start.10
  37.9 1.1 copy-start.7
  38.9 164.1 %reduce-scatter.2.cloned.1.call-start = ((), (), s32[]{:S(2)}) async-start(), calls=%async_computation.3 | async-start | bytes 2621440 | tf_op jit(solution)/shard_map/reduce_scatter | solution.py:177
  40.4 2.8 %copy-start.4 = (bf16[512,2048]{1,0:T(8,128)(2,1)S(1)}, bf16[512,2048]{1,0:T(8,128)(2,1)}, u32[]{:S(2)}) copy-start(bf16[512,2048]{1,0:T(8,128)(2,1)} %all-gather.3.cloned.1.call-done) | copy-start | bytes 6291460
  40.4 2.8 %copy-start.12 = (bf16[2048,256]{1,0:T(8,128)(2,1)S(1)}, bf16[2048,256]{1,0:T(8,128)(2,1)}, u32[]{:S(2)}) copy-start(bf16[2048,256]{1,0:T(8,128)(2,1)} %param.22) | copy-start | bytes 3145732
  43.2 6.3 %copy-start.13 = (bf16[2048,64]{0,1:T(8,128)(2,1)S(1)}, bf16[2048,64]{0,1:T(8,128)(2,1)}, u32[]{:S(2)}) copy-start(bf16[2048,64]{0,1:T(8,128)(2,1)} %param.28) | copy-start | bytes 786436
  44.6 44.7 %collective-permute-start = (bf16[15,256]{1,0:T(8,128)(2,1)}, bf16[15,256]{1,0:T(8,128)(2,1)S(1)}, u32[]{:S(2)}, u32[]{:S(2)}) collective-permute-start(bf16[15,256]{1,0:T(8,128)(2,1)} %get-tuple-element.134), channel_id=1, source_target_pairs={{0,4},{4,8},{8,12},{12,16},{16,20},{20,24},{24,28},{1,5},{5,9},{9,... | collective-permute-start | bytes 23048 | tf_op jit(solution)/shard_map/ppermute | solution.py:25
  48.0 2.7 %copy-start.11 = (bf16[2048,512]{1,0:T(8,128)(2,1)S(1)}, bf16[2048,512]{1,0:T(8,128)(2,1)}, u32[]{:S(2)}) copy-start(bf16[2048,512]{1,0:T(8,128)(2,1)} %param.26) | copy-start | bytes 6291460
  48.0 2.7 %copy-start.15 = (f32[2048]{0:T(1024)S(1)}, f32[2048]{0:T(1024)}, u32[]{:S(2)}) copy-start(f32[2048]{0:T(1024)} %param.21) | copy-start | bytes 24580
  48.0 41.3 %collective-permute-start.1 = (bf16[15,256]{1,0:T(8,128)(2,1)}, bf16[15,256]{1,0:T(8,128)(2,1)}, u32[]{:S(2)}, u32[]{:S(2)}) collective-permute-start(bf16[15,256]{1,0:T(8,128)(2,1)} %get-tuple-element.135), channel_id=1, source_target_pairs={{4,0},{8,4},{12,8},{16,12},{20,16},{24,20},{28,24},{5,1},{9,5},{13... | collective-permute-start | bytes 23048 | tf_op jit(solution)/shard_map/ppermute | solution.py:26
  50.7 36.8 %copy-start.6 = (bf16[512,128]{1,0:T(8,128)(2,1)S(1)}, bf16[512,128]{1,0:T(8,128)(2,1)}, u32[]{:S(2)}) copy-start(bf16[512,128]{1,0:T(8,128)(2,1)} %param.32) | copy-start | bytes 393220
  50.7 36.7 %copy-start.9 = (f32[512]{0:T(512)S(1)}, f32[512]{0:T(512)}, u32[]{:S(2)}) copy-start(f32[512]{0:T(512)} %param.29) | copy-start | bytes 6148
  52.2 35.7 %copy-start.5 = (bf16[512,256]{1,0:T(8,128)(2,1)S(1)}, bf16[512,256]{1,0:T(8,128)(2,1)}, u32[]{:S(2)}) copy-start(bf16[512,256]{1,0:T(8,128)(2,1)} %param.31) | copy-start | bytes 786436
  105.0 19.1 %copy-start.1 = (bf16[512,256]{1,0:T(8,128)(2,1)S(1)}, bf16[512,256]{1,0:T(8,128)(2,1)}, u32[]{:S(2)}) copy-start(bf16[512,256]{1,0:T(8,128)(2,1)} %param.33) | copy-start | bytes 786436
  105.0 19.1 %copy-start.2 = (bf16[512,256]{1,0:T(8,128)(2,1)S(1)}, bf16[512,256]{1,0:T(8,128)(2,1)}, u32[]{:S(2)}) copy-start(bf16[512,256]{1,0:T(8,128)(2,1)} %param.34) | copy-start | bytes 786436
  173.1 31.1 %copy-start.8 = (f32[2048]{0:T(1024)S(1)}, f32[2048]{0:T(1024)}, u32[]{:S(2)}) copy-start(f32[2048]{0:T(1024)} %param.37) | copy-start | bytes 24580
Sparse Core Ops, SparseCore 0:
  8.9 25.2 all-gather.2
  39.1 78.5 all-gather.4
  173.3 29.7 reduce-scatter.1
where the time goes:
time: 214 us; the launch traced here: 213 us
  waiting for transfers between devices  70.2 us (33%)
  matrix products  57.8 us (27%)
  blocking collectives  42.1 us (20%)
  other arithmetic  14.4 us (7%)
  between operations  13.5 us (6%)
  local copies, waits for them, and re-layouts  9.48 us (4%)
  starting transfers between devices  4.89 us (2%)
    all_gather x1, blocking collectives, local(): lax.all_gather(rope_keys, 'sp', axis=0, tiled=True)  35.2 us
    reduce_scatter x1, waiting for transfers between devices, local(): lax.psum_scatter(lax.optimization_barrier(summed.astype(jnp.bfloat16)).as...  29.9 us
    all_gather x1, waiting for transfers between devices, local(): full_rows = lax.all_gather(tokens, 'tp', axis=1, tiled=True)  26.9 us
    all_gather x1, waiting for transfers between devices, local(): lax.all_gather(latent, 'sp', axis=0, tiled=True)  12.6 us
    dot_general x8, matrix products, block_step(): jnp.dot(latent_rows, key_weight, preferred_element_type=jnp.float32)  11.1 us
    dot_general x8, matrix products, block_step(): jnp.dot(latent_rows, value_weight, preferred_element_type=jnp.float32)  11.1 us
    dot_general x8, matrix products, attend(): jnp.einsum('thr,pr->htp', query_rope, rope_rows, preferred_element_type=j...  10.5 us
    psum x1, blocking collectives, local(): lax.psum((jnp.sum(convolved, axis=1), jnp.sum(convolved * convolved, axis...  6.83 us
  transfers between devices with their start and end apart: 5, of which 3 were waited for; matrix products, arithmetic and copies ran while one was open for 9% of the time, Pallas kernels for 0%

commit v1 on v0

v1 whole, which is shorter than its diff:
```python
import functools

import jax
import jax.numpy as jnp
from jax import lax
from jax.experimental import pallas as pl
from jax.experimental.pallas import tpu as pltpu
from jax.sharding import PartitionSpec as P

HEAD_WIDTH = 128
norm_eps = 1e-06
layer_eps = 1e-05
rope_base = 10000.0
CHUNKS = 4
MESH = pl.DeviceIdType.MESH
F32 = jnp.float32
BF16 = jnp.bfloat16


def dot(a, b):
    return jnp.dot(a, b, preferred_element_type=F32)


def dot_nt(a, b):
    return lax.dot_general(a, b, (((1,), (1,)), ((), ())), preferred_element_type=F32)


def rms(values, gain):
    return values * lax.rsqrt(jnp.mean(values * values, axis=-1, keepdims=True) + norm_eps) * gain


def rotate_pair(values, cosine, sine):
    lane = lax.broadcasted_iota(jnp.int32, values.shape, 1)
    swapped = jnp.where(
        lane % 64 < 32, pltpu.roll(values, 96, 1), pltpu.roll(values, 32, 1)
    )
    return values * cosine + swapped * sine


def layer(
    cfg,
    tokens, in_gain, cvw, cgw, taps, conv_gain, qlw, lw, rkw, q_gain, l_gain,
    qw, qrw, kw, vw, cow, aow, out_gain, cosine, sine,
    out,
    xb, v_cvw, v_cgw, v_qlw, v_lw, v_rkw, v_qw, v_qrw, v_kw, v_vw, v_cow, v_aow,
    nb, kvb, halo_s, halo_r, pad, conv, st_col, st_s, st_r, crs, qs, mx, acc, ars,
    psb, pr, pa, xr,
    tok_sem, w_sem, xs_send, xs_fwd, xs_recv, g_recv, g_zs, g_ys, g_ps,
    h_send, h_recv, t_send, t_recv, p_send, p_recv, r_send, r_recv,
):
    S, TP, Z, Y, X, T, F, D, C, H = cfg
    R = T // CHUNKS
    Tb = T // TP
    s = lax.axis_index("sp")
    t = lax.axis_index("tp")
    z, y = s // Y, s % Y
    x, c = t // 2, t % 2
    mate = x * 2 + (1 - c)

    def remote(src, dst, ss, rs, dev):
        return pltpu.make_async_remote_copy(
            src_ref=src, dst_ref=dst, send_sem=ss, recv_sem=rs, device_id=dev, device_id_type=MESH
        )

    tok_copies = [
        pltpu.make_async_copy(
            tokens.at[pl.ds(r * R, R), :], xb.at[t, pl.ds(r * R, R), :], tok_sem.at[r]
        )
        for r in range(CHUNKS)
    ]
    pairs = [
        (lw, v_lw), (rkw, v_rkw), (cvw, v_cvw), (cgw, v_cgw), (qlw, v_qlw), (qw, v_qw),
        (qrw, v_qrw), (kw, v_kw), (vw, v_vw), (cow, v_cow), (aow, v_aow),
    ]
    w_copies = [pltpu.make_async_copy(a, b, w_sem.at[i]) for i, (a, b) in enumerate(pairs)]
    for cp in tok_copies + w_copies:
        cp.start()

    barrier = pltpu.get_barrier_semaphore()
    peers = [(s, (t + e) % TP) for e in range(1, TP)]
    peers += [(((z + e) % Z) * Y + y, t) for e in (1, Z - 1)]
    peers += [(z * Y + (y + e) % Y, t) for e in range(1, Y)]
    peers += [((s + e) % S, t) for e in (1, S - 1)]
    for dev in peers:
        pl.semaphore_signal(barrier, inc=1, device_id=dev, device_id_type=MESH)
    pl.semaphore_wait(barrier, len(peers))

    def tok_copy(src, r, ss, dev):
        blk = xb.at[src, pl.ds(r * R, R), :]
        return remote(blk, blk, ss, xs_recv.at[src, r], dev)

    own_sends = []
    for r in range(CHUNKS):
        tok_copies[r].wait()
        for e in range(1, X):
            cp = tok_copy(t, r, xs_send.at[e, r], (s, ((x + e) % X) * 2 + c))
            cp.start()
            own_sends.append(cp)
        cp = tok_copy(t, r, xs_send.at[0, r], (s, mate))
        cp.start()
        own_sends.append(cp)

    def slot(src, r):
        return kvb.at[src, r]

    def z_copy(zs, i, up):
        src, r = zs * Y + y, c + 2 * i
        step = 1 if up else -1
        return remote(
            slot(src, r), slot(src, r), g_zs.at[0 if up else 1, zs, i], g_recv.at[src, r],
            ((z + step) * Y + y, t),
        )

    def y_copy(zs, i, e):
        src, r = zs * Y + y, c + 2 * i
        return remote(
            slot(src, r), slot(src, r), g_ys.at[e - 1, zs, i], g_recv.at[src, r],
            (z * Y + (y + e) % Y, t),
        )

    def mate_copy(src, i):
        r = c + 2 * i
        return remote(
            slot(src, r), slot(src, r), g_ps.at[src, i], g_recv.at[src, r], (s, mate)
        )

    def arrived(src, r):
        remote(
            slot(src, r), slot(src, r), g_ps.at[src, 0], g_recv.at[src, r], (s, mate)
        ).wait_recv()

    def relay(d, i):
        lo, hi = z - d, z + d

        @pl.when(lo >= 0)
        def _():
            arrived(lo * Y + y, c + 2 * i)

            @pl.when(z + 1 < Z)
            def _():
                z_copy(lo, i, True).start()

            for e in range(1, Y):
                y_copy(lo, i, e).start()
            mate_copy(lo * Y + y, i).start()

        @pl.when(hi < Z)
        def _():
            arrived(hi * Y + y, c + 2 * i)

            @pl.when(z - 1 >= 0)
            def _():
                z_copy(hi, i, False).start()

            for e in range(1, Y):
                y_copy(hi, i, e).start()
            mate_copy(hi * Y + y, i).start()

    fwd_sends = []
    lane = lax.broadcasted_iota(jnp.int32, (R // 8, 128), 1)
    for r in range(CHUNKS):
        rows = pl.ds(r * R, R)
        for e in range(1, X):
            src = ((x + e) % X) * 2 + c
            tok_copy(src, r, xs_send.at[e, r], (s, mate)).wait_recv()
            cp = tok_copy(src, r, xs_fwd.at[e - 1, r], (s, mate))
            cp.start()
            fwd_sends.append(cp)
        for e in range(X):
            src = ((x + e) % X) * 2 + (1 - c)
            tok_copy(src, r, xs_send.at[0, r], (s, mate)).wait_recv()
        total = jnp.zeros((R, 1), F32)
        for g in range(TP):
            v = xb[g, rows, :].astype(F32)
            total += jnp.sum(v * v, axis=1, keepdims=True)
        scale = lax.rsqrt(total / D + norm_eps)
        for g in range(TP):
            cols = slice(g * F, (g + 1) * F)
            nb[rows, cols] = (xb[g, rows, :].astype(F32) * scale * in_gain[:, cols]).astype(BF16)
        if r == 0:
            w_copies[0].wait()
            w_copies[1].wait()
        n = nb[rows, :]
        kvb[s, r, 0:R, :] = rms(dot(n, v_lw[...]), l_gain[...]).astype(BF16)
        rk = rotate_pair(dot(n, v_rkw[...]), cosine[rows, :], sine[rows, :])
        per = R // 8
        for k in range(4):
            kvb[s, r, R : R + per, 128 * k : 128 * (k + 1)] = jnp.where(
                lane < 64, rk[2 * per * k : 2 * per * k + per], rk[2 * per * k + per : 2 * per * (k + 1)]
            ).astype(BF16)

        @pl.when(c == r % 2)
        def _():
            i = r // 2
            src = z * Y + y

            @pl.when(z + 1 < Z)
            def _():
                z_copy(z, i, True).start()

            @pl.when(z - 1 >= 0)
            def _():
                z_copy(z, i, False).start()

            for e in range(1, Y):
                y_copy(z, i, e).start()

        if r == 2:
            relay(1, 0)

    for k in (2, 3):
        w_copies[k].wait()
    for q in range(2):
        rows = pl.ds(q * (T // 2), T // 2)
        n = nb[rows, :]
        cv = dot(n, v_cvw[...])
        cg = dot(n, v_cgw[...])
        gated = (cv * jax.nn.sigmoid(cg)).astype(BF16)
        if q == 0:
            halo_s[0] = gated[0:16]
        else:
            halo_s[1] = gated[T // 2 - 16 :]
        gf = gated.astype(F32)
        for l in range(C // 128):
            pad[l, 16 + q * (T // 2) : 16 + (q + 1) * (T // 2), :] = gf[:, 128 * l : 128 * (l + 1)]

    def halo(up):
        k = 1 if up else 0
        return remote(
            halo_s.at[k], halo_r.at[1 - k], h_send.at[k], h_recv.at[1 - k],
            (s + 1 if up else s - 1, t),
        )

    @pl.when(s > 0)
    def _():
        halo(False).start()

    @pl.when(s < S - 1)
    def _():
        halo(True).start()

    relay(1, 1)

    for k in (4, 5, 6):
        w_copies[k].wait()
    for q in range(2):
        rows = pl.ds(q * (T // 2), T // 2)
        ql = rms(dot(nb[rows, :], v_qlw[...]), q_gain[...]).astype(BF16)
        qm = dot(ql, v_qw[...])
        qr = dot(ql, v_qrw[...])
        half = lax.broadcasted_iota(jnp.int32, (T // 2, 128), 1) < 64
        for h in range(H):
            hs = slice(128 * h, 128 * (h + 1))
            qs[h, rows, 0:128] = qm[:, hs].astype(BF16)
            rot = rotate_pair(qr[:, hs], cosine[rows, :], sine[rows, :])
            qs[h, rows, 128:256] = jnp.where(half, rot, 0.0).astype(BF16)

    relay(2, 0)

    @pl.when(s > 0)
    def _():
        remote(halo_s.at[1], halo_r.at[0], h_send.at[1], h_recv.at[0], (s - 1, t)).wait_recv()
        for l in range(C // 128):
            pad[l, 0:16, :] = halo_r[0, :, 128 * l : 128 * (l + 1)].astype(F32)

    @pl.when(s == 0)
    def _():
        for l in range(C // 128):
            pad[l, 0:16, :] = jnp.zeros((16, 128), F32)

    @pl.when(s < S - 1)
    def _():
        remote(halo_s.at[0], halo_r.at[1], h_send.at[0], h_recv.at[1], (s + 1, t)).wait_recv()
        for l in range(C // 128):
            pad[l, T + 16 : T + 32, :] = halo_r[1, :, 128 * l : 128 * (l + 1)].astype(F32)

    @pl.when(s == S - 1)
    def _():
        for l in range(C // 128):
            pad[l, T + 16 : T + 32, :] = jnp.zeros((16, 128), F32)

    K = taps.shape[0]
    B = 64

    def conv_tile(i, carry):
        base = i * B
        s1 = jnp.zeros((B, 128), F32)
        s2 = jnp.zeros((B, 128), F32)
        for l in range(C // 128):
            a = jnp.zeros((B, 128), F32)
            for j in range(K):
                off = 16 - K // 2 + j
                a += taps[j : j + 1, 128 * l : 128 * (l + 1)] * pad[l, pl.ds(base + off, B), :]
            conv[pl.ds(pl.multiple_of(base, B), B), 128 * l : 128 * (l + 1)] = a
            s1 += a
            s2 += a * a
        lanes = lax.broadcasted_iota(jnp.int32, (B, 128), 1)
        r1 = jnp.sum(s1, axis=1, keepdims=True)
        r2 = jnp.sum(s2, axis=1, keepdims=True)
        st_col[pl.ds(pl.multiple_of(base, B), B), :] = jnp.where(
            lanes == 0, r1, jnp.where(lanes == 1, r2, 0.0)
        )
        return carry

    lax.fori_loop(0, T // B, conv_tile, 0)
    st_s[...] = jnp.transpose(st_col[...])[0:8]
    st_sends = []
    for e in range(1, TP):
        cp = remote(
            st_s, st_r.at[e - 1], t_send.at[e - 1], t_recv.at[e - 1], (s, (t + e) % TP)
        )
        cp.start()
        st_sends.append(cp)

    relay(2, 1)

    scale2 = (HEAD_WIDTH + 64) ** (-0.5) * 1.4426950408889634
    mx[...] = jnp.full(mx.shape, -1e30, F32)
    acc[...] = jnp.zeros(acc.shape, F32)
    for k in (7, 8):
        w_copies[k].wait()
    QB = T // 2

    def attend(src):
        lat = kvb[src, :, 0:R, :].reshape(T, kvb.shape[3])
        k = dot(lat, v_kw[...]).astype(BF16)
        v = dot(lat, v_vw[...]).astype(BF16)
        ropes = []
        for r in range(CHUNKS):
            for g in range(4):
                tile = kvb[src, r, R:, 128 * g : 128 * (g + 1)].astype(F32)
                turned = pltpu.roll(tile, 64, 1)
                ropes.append(jnp.where(lane < 64, tile, turned).astype(BF16))
                ropes.append(jnp.where(lane < 64, turned, tile).astype(BF16))
        rope = jnp.concatenate(ropes, axis=0)
        ones = jnp.ones((T, 128), BF16)
        for h in range(H):
            hs = slice(128 * h, 128 * (h + 1))
            kc = jnp.concatenate([k[:, hs], rope], axis=1)
            vc = jnp.concatenate([v[:, hs], ones], axis=1)
            for qb in range(T // QB):
                rows = slice(qb * QB, (qb + 1) * QB)
                sc = dot_nt(qs[h, rows, :], kc)
                old = mx[h, rows, :]
                new = jnp.maximum(old, jnp.max(sc, axis=1, keepdims=True))
                mx[h, rows, :] = new
                alpha = jnp.exp2((old - new) * scale2)
                p = jnp.exp2((sc - new[:, 0:1]) * scale2).astype(BF16)
                acc[h, rows, :] = acc[h, rows, :] * jnp.concatenate([alpha, alpha], axis=1) + dot(p, vc)

    def key_step(d, carry):
        zd = jnp.where(z < Z // 2, lax.rem(z + d, Z), lax.rem(z - d + Z, Z))

        @pl.when(d > 0)
        def _():
            for i in range(CHUNKS // 2):
                arrived(zd * Y + y, (1 - c) + 2 * i)

        attend(zd * Y + y)

        @pl.when(d + 3 < Z)
        def _():
            relay(d + 3, 0)

        def across(e, carry2):
            src = zd * Y + lax.rem(y + e, Y)
            for i in range(CHUNKS // 2):
                arrived(src, c + 2 * i)
                mate_copy(src, i).start()
            for i in range(CHUNKS // 2):
                arrived(src, (1 - c) + 2 * i)
            attend(src)
            return carry2

        lax.fori_loop(1, Y, across, 0)

        @pl.when(d + 3 < Z)
        def _():
            relay(d + 3, 1)

        return carry

    sums = st_s[...]
    for e in range(1, TP):
        remote(
            st_s, st_r.at[e - 1], t_send.at[e - 1], t_recv.at[e - 1], (s, (t + e) % TP)
        ).wait_recv()
        sums += st_r[e - 1]
    cols = jnp.transpose(jnp.concatenate([sums] * 16, axis=0))
    mean = cols[:, 0:1] / (C * TP)
    square = cols[:, 1:2] / (C * TP)
    inv = lax.rsqrt(square - mean * mean + layer_eps)
    shaped = (conv[...] - mean) * inv * conv_gain[...]
    crs[...] = (shaped * jax.nn.sigmoid(shaped)).astype(BF16)

    lax.fori_loop(0, Z, key_step, 0)

    for h in range(H):
        ars[:, 128 * h : 128 * (h + 1)] = (acc[h, :, 0:128] / acc[h, :, 128:256]).astype(BF16)

    for k in (9, 10):
        w_copies[k].wait()
    NC = psb.shape[-1]
    NCH = D // NC

    def to_mate(n):
        return remote(psb.at[n, 1 - c], pr.at[n], p_send.at[n], p_recv.at[n], (s, mate))

    def across_chips(n, e):
        return remote(
            pa.at[n, e - 1], xr.at[n, e - 1], r_send.at[n, e - 1], r_recv.at[n, e - 1],
            (s, ((x + e) % X) * 2 + c),
        )

    def pair_sum(n):
        to_mate(n).wait_recv()
        for e in range(1, X):
            xd = (x + e) % X
            pa[n, e - 1] = (psb[n, c, xd].astype(F32) + pr[n, xd].astype(F32)).astype(BF16)
            across_chips(n, e).start()

    for n in range(NCH):
        cs = slice(n * NC, (n + 1) * NC)
        part = (dot(crs[...], v_cow[:, cs]) + dot(ars[...], v_aow[:, cs])).astype(BF16)
        for g in range(TP):
            psb[n, g % 2, g // 2] = part[g * Tb : (g + 1) * Tb]
        to_mate(n).start()
        if n > 0:
            pair_sum(n - 1)
    pair_sum(NCH - 1)

    merged = []
    square_sum = jnp.zeros((Tb, 1), F32)
    for n in range(NCH):
        m = psb[n, c, x].astype(F32) + pr[n, x].astype(F32)
        for e in range(1, X):
            across_chips(n, e).wait_recv()
            m += xr[n, e - 1].astype(F32)
        square_sum += jnp.sum(m * m, axis=1, keepdims=True)
        merged.append(m)
    inv_out = lax.rsqrt(square_sum / D + norm_eps)
    for n in range(NCH):
        cs = slice(n * NC, (n + 1) * NC)
        out[:, cs] = (merged[n] * inv_out * out_gain[:, cs]).astype(BF16)

    for cp in own_sends + fwd_sends + st_sends:
        cp.wait_send()

    @pl.when(s > 0)
    def _():
        halo(False).wait_send()

    @pl.when(s < S - 1)
    def _():
        halo(True).wait_send()

    def drain(zs, carry):
        for i in range(CHUNKS // 2):

            @pl.when((zs <= z) & (z + 1 < Z))
            def _():
                z_copy(zs, i, True).wait_send()

            @pl.when((zs >= z) & (z - 1 >= 0))
            def _():
                z_copy(zs, i, False).wait_send()

            for e in range(1, Y):
                y_copy(zs, i, e).wait_send()
                mate_copy(zs * Y + lax.rem(y + e, Y), i).wait_send()

            @pl.when(zs != z)
            def _():
                mate_copy(zs * Y + y, i).wait_send()

        return carry

    lax.fori_loop(0, Z, drain, 0)
    for n in range(NCH):
        to_mate(n).wait_send()
        for e in range(1, X):
            across_chips(n, e).wait_send()


def local(S, TP, *args):
    (tokens, in_gain, cvw, cgw, taps, conv_gain, qlw, lw, rkw, q_gain, l_gain,
     qw, qrw, kw, vw, cow, aow, out_gain) = args
    T, F = tokens.shape
    D = F * TP
    C = cvw.shape[1]
    H = kw.shape[1] // HEAD_WIDTH
    QL, L = qlw.shape[1], lw.shape[1]
    RW = rkw.shape[1]
    Y = 1
    while 2 * (2 * Y) ** 2 <= S:
        Y *= 2
    Z, X = S // Y, TP // 2
    cfg = (S, TP, Z, Y, X, T, F, D, C, H)
    R = T // CHUNKS
    Tb = T // TP
    NC = D // 4

    positions = (lax.axis_index("sp") * T + jnp.arange(T, dtype=jnp.int32)).astype(F32)
    half = RW // 2
    inverse = rope_base ** (-jnp.arange(half, dtype=F32) / half)
    angles = positions[:, None] * inverse[None, :]
    co, si = jnp.cos(angles), jnp.sin(angles)
    cosine = jnp.concatenate([co] * 4, axis=1)
    sine = jnp.concatenate([-si, si] * 2, axis=1)
    rkw2 = jnp.concatenate([rkw, rkw], axis=1)
    q3 = qrw.reshape(QL, H, RW)
    qrw2 = jnp.concatenate([q3, q3], axis=2).reshape(QL, H * 2 * RW)

    row = lambda v: v.reshape(1, -1)
    hbm = pl.BlockSpec(memory_space=pl.ANY)
    vm = pl.BlockSpec(memory_space=pltpu.VMEM)
    V = pltpu.VMEM
    sem = pltpu.SemaphoreType.DMA
    return pl.pallas_call(
        functools.partial(layer, cfg),
        out_shape=jax.ShapeDtypeStruct((Tb, D), BF16),
        in_specs=[hbm, vm, hbm, hbm, vm, vm, hbm, hbm, hbm, vm, vm,
                  hbm, hbm, hbm, hbm, hbm, hbm, vm, vm, vm],
        out_specs=vm,
        scratch_shapes=[
            V((TP, T, F), BF16),
            V((D, C), BF16), V((D, C), BF16), V((D, QL), BF16), V((D, L), BF16),
            V((D, 2 * RW), BF16), V((QL, H * 128), BF16), V((QL, H * 128), BF16),
            V((L, H * 128), BF16), V((L, H * 128), BF16), V((C, D), BF16), V((H * 128, D), BF16),
            V((T, D), BF16),
            V((S, CHUNKS, R + R // 8, L), BF16),
            V((2, 16, C), BF16), V((2, 16, C), BF16),
            V((C // 128, T + 32, 128), F32), V((T, C), F32),
            V((T, 128), F32), V((8, T), F32), V((TP - 1, 8, T), F32),
            V((T, C), BF16),
            V((H, T, 256), BF16), V((H, T, 128), F32), V((H, T, 256), F32),
            V((T, H * 128), BF16),
            V((4, 2, X, Tb, NC), BF16), V((4, X, Tb, NC), BF16),
            V((4, X - 1, Tb, NC), BF16), V((4, X - 1, Tb, NC), BF16),
            sem((CHUNKS,)), sem((11,)), sem((X, CHUNKS)), sem((X - 1, CHUNKS)), sem((TP, CHUNKS)),
            sem((S, CHUNKS)), sem((2, Z, CHUNKS // 2)), sem((Y - 1, Z, CHUNKS // 2)),
            sem((S, CHUNKS // 2)),
            sem((2,)), sem((2,)), sem((TP - 1,)), sem((TP - 1,)),
            sem((4,)), sem((4,)), sem((4, X - 1)), sem((4, X - 1)),
        ],
        compiler_params=pltpu.CompilerParams(
            collective_id=0, has_side_effects=True, vmem_limit_bytes=67043328
        ),
    )(
        tokens, row(in_gain), cvw, cgw, taps, row(conv_gain), qlw, lw, rkw2, row(q_gain),
        row(l_gain), qw, qrw2, kw, vw, cow, aow, row(out_gain), cosine, sine,
    )


def solution(mesh):
    sizes = mesh.shape
    return jax.shard_map(
        functools.partial(local, sizes["sp"], sizes["tp"]),
        mesh=mesh,
        in_specs=(
            P("sp", "tp"), P(), P(None, "tp"), P(None, "tp"), P(None, "tp"), P("tp"),
            P(), P(), P(), P(), P(),
            P(None, "tp"), P(None, "tp"), P(None, "tp"), P(None, "tp"),
            P("tp", None), P("tp", None), P(),
        ),
        out_specs=P(("sp", "tp"), None),
        check_vma=False,
    )
```

time: 214 us -> 78.2 us (0.37)
  Pallas kernels: 0 us -> 71.5 us
  waiting for transfers between devices: 70.2 us -> 0 us
  matrix products: 57.8 us -> 0 us
  blocking collectives: 42.1 us -> 0 us
  between operations: 13.5 us -> 0.04 us
  other arithmetic: 14.4 us -> 3.39 us
  local copies, waits for them, and re-layouts: 9.48 us -> 3.1 us
  starting transfers between devices: 4.89 us -> 0 us
    pallas_call x0 -> x1, Pallas kernels: none -> 71.5 us  [local(): pl.pallas_call(functools.partial(layer, cfg), out_shape=jax.ShapeDtypeStr...]
    dot_general x49 -> x0, matrix products: 57.8 us -> none  [the longest x8 11.1 us: block_step(): jnp.dot(latent_rows, key_weight, preferred_element_type=jnp.float32)]
    all_gather x2 -> x0, waiting for transfers between devices: 39.5 us -> none  [the longest x1 26.9 us: local(): full_rows = lax.all_gather(tokens, 'tp', axis=1, tiled=True)]
    all_gather x1 -> x0, blocking collectives: 35.2 us -> none  [local(): lax.all_gather(rope_keys, 'sp', axis=0, tiled=True)]
    reduce_scatter x1 -> x0, waiting for transfers between devices: 29.9 us -> none  [local(): lax.psum_scatter(lax.optimization_barrier(summed.astype(jnp.bfloat16)).as...]
    reduce_sum x11 -> x0, other arithmetic: 9.21 us -> none  [the longest x2 3.45 us: rms_scaled(): jnp.mean(values * values, axis=-1, keepdims=True) + norm_eps]
    psum x1 -> x0, blocking collectives: 6.83 us -> none  [local(): lax.psum((jnp.sum(convolved, axis=1), jnp.sum(convolved * convolved, axis...]
    ppermute x2 -> x0, starting transfers between devices: 4.81 us -> none  [the longest x1 3.39 us: extended(): before = lax.ppermute(last, axis, up)]
  transfers between devices with their start and end apart: 5 -> 0, of which waited for: 3 -> 0; matrix products, arithmetic and copies ran while one was open for 9% -> 0% of each run, Pallas kernels for 0% -> 0%
where the time goes in v1:
time: 78.2 us; the launch traced here: 78.1 us
  Pallas kernels  71.5 us (91%)
  other arithmetic  3.39 us (4%)
  local copies, waits for them, and re-layouts  3.1 us (4%)
    pallas_call x1, Pallas kernels, local(): pl.pallas_call(functools.partial(layer, cfg), out_shape=jax.ShapeDtypeStr...  71.5 us
    unnamed x7, local copies, waits for them, and re-layouts  2.27 us

profile of v1, /device:TPU:0, one launch (start us, length us, event | category | flops | bytes accessed | tf_op | source)
XLA Modules:
  0.0 78.1 jit_solution(1157361633587448901)
XLA Ops:
  0.0 0.0 copy-start
  0.0 0.0 copy-start.1
  0.0 1.0 %fusion = (f32[512,32]{1,0:T(8,128)S(1)}, f32[512,32]{1,0:T(8,128)S(1)}, f32[512,32]{1,0:T(8,128)S(1)}) fusion(f32[32]{0:T(128)S(1)} %multiply_power_fusion, f32[512]{0:T(512)S(1)} %add_convert_fusion), kind=kLoop, calls=%fused_computation.6 | loop fusion | flops 32768 | bytes 198784 | tf_op jit(solution)/shard_map/neg | solution.py:509
  1.0 1.3 %pad_maximum_fusion.2 = (f32[512,128]{1,0:T(8,128)}, f32[512,128]{1,0:T(8,128)}) fusion(f32[512,32]{1,0:T(8,128)S(1)} %get-tuple-element.7, f32[512,32]{1,0:T(8,128)S(1)} %get-tuple-element.6, f32[512,32]{1,0:T(8,128)S(1)} %get-tuple-element.5), kind=kLoop, calls=%fused_computation.4 | loop fusion | flops 393216 | bytes 720896 | tf_op jit(solution)/shard_map/concatenate | solution.py:508
  2.3 0.0 copy-done
  2.3 0.3 copy.25
  2.6 1.1 %pad_maximum_fusion.rkw = bf16[2048,128]{1,0:T(8,128)(2,1)} fusion(bf16[2048,64]{1,0:T(8,128)(2,1)S(1)} %copy.25), kind=kLoop, calls=%fused_computation | loop fusion | flops 1048576 | bytes 786432 | tf_op jit(solution)/shard_map/concatenate | solution.py:510
  3.7 0.0 copy-done.1
  3.7 0.1 copy.27
  3.8 0.8 %copy.30.qrw = bf16[512,256]{1,0:T(8,128)(2,1)} copy(bf16[512,256]{0,1:T(8,128)(2,1)S(1)} %bitcast.7) | data formatting | bytes 524288 | tf_op jit(solution)/shard_map/reshape | solution.py:512
  4.6 71.5 %shard_map.172 = bf16[128,2048]{1,0:T(8,128)(2,1)} custom-call(bf16[512,512]{1,0:T(8,128)(2,1)} %tokens.1, f32[1,2048]{1,0:T(1,128)} %bitcast.9, bf16[2048,256]{1,0:T(8,128)(2,1)} %cvw.1, bf16[2048,256]{1,0:T(8,128)(2,1)} %cgw.1, f32[31,256]{1,0:T(8,128)} %taps.1, f32[1,256]{1,0:T(1,128)} %bitcast.13, bf16[2048,512]{1,0:T(8,128)(2,1)} %qlw.1, ...), custom_call_target="tpu_custom_call" | custom-call | tf_op jit(solution)/shard_map/pallas_call | solution.py:519
  76.2 1.9 %copy.32 = bf16[128,2048]{1,0:T(8,128)(2,1)} copy(bf16[128,2048]{1,0:T(8,128)(2,1)} %shard_map.172) | data formatting | bytes 1048576
  (3 shorter events, 0.0 us)
Async XLA Ops:
  0.0 2.3 %copy-start = (bf16[2048,64]{0,1:T(8,128)(2,1)S(1)}, bf16[2048,64]{0,1:T(8,128)(2,1)}, u32[]{:S(2)}) copy-start(bf16[2048,64]{0,1:T(8,128)(2,1)} %param.26) | copy-start | bytes 786436
  0.0 3.7 %copy-start.1 = (bf16[512,128]{1,0:T(8,128)(2,1)S(1)}, bf16[512,128]{1,0:T(8,128)(2,1)}, u32[]{:S(2)}) copy-start(bf16[512,128]{1,0:T(8,128)(2,1)} %param.30) | copy-start | bytes 393220
